TPU v7x, 512 devices: a 4x2x32 block of a 4x8x32 slice. The times are simulated.
512 devices in a mesh: grp: 2 (over y), ep: 64 (over z, core), tp: 4 (over x).
Axes of the slice: x: 4, y: 2, z: 32, core: 2. Of those that a mesh axis runs over, the one named last changes fastest.
The devices are a block of a 4x8x32 slice.
Arguments:
- tokens: bfloat16 [24576, 2048], P(('grp', 'ep')), parts along dimension 0, may hold values from -6 to 6
- norm_gain: float32 [2048], replicated, may hold values from 0.1 to 1.9
- w_gate: bfloat16 [64, 2048, 1024], P('ep', None, 'tp'), may hold values from -0.3125 to 0.3125
- w_up: bfloat16 [64, 2048, 1024], P('ep', None, 'tp'), may hold values from -0.3125 to 0.3125
- w_down: bfloat16 [64, 1024, 2048], P('ep', 'tp'), may hold values from -0.09375 to 0.09375
- expert_ids: int32 [24576, 4], P(('grp', 'ep')), parts along dimension 0, may hold values from 0 to 63, all different within a row; in each aligned block of 192 rows (0 to 191, 192 to 383, ...) at most 16 rows name the same one
- gate_weights: float32 [24576, 4], P(('grp', 'ep')), parts along dimension 0, may hold values from 0.1 to 1
Outputs:
- mixed: bfloat16 [24576, 2048], P(('grp', 'ep'), 'tp'), parts along dimension 0
There are 2 independent parts, one for each index of `grp`. A program takes and returns all parts, laid end to end along the dimension named above; an argument that names none is the same for every part. Nothing has to cross between parts.
Inputs may be any that keep to these rules, and one draw needn't show every extreme that they name: `expert_ids`: each row names 4 different experts; among the rows of one index of ep, no expert is named by more than 16 rows, a bound that some block reaches.
All inputs are finite; a program needn't handle non-finite values.
Results may differ from a plain program's by a relative error of at most 0.012.
Values may be sent and summed in bfloat16 or wider, within the bound.
A program may use at most 64 MiB of HBM per device.

v0:
```python
import jax
import jax.numpy as jnp
from jax import lax
from jax.sharding import Mesh
from jax.sharding import PartitionSpec as P

EP = ("ep_0", "ep_1")
GRP_EP = ("grp", "ep_0", "ep_1")


epsilon = 1e-06
clamp_limit = 7.0
swish_alpha = 1.702


def cut_along(value, dim, devices):
    before, after = (value.shape[:dim], value.shape[dim + 1 :])
    return jnp.moveaxis(value.reshape(*before, devices, -1, *after), dim, 0)


def laid_out(blocks, dim):
    blocks = jnp.moveaxis(blocks, 0, dim)
    shape = blocks.shape
    return blocks.reshape(*shape[:dim], shape[dim] * shape[dim + 1], *shape[dim + 2 :])


def turned_blocks(blocks, axes, turns):
    inside = blocks.shape[1:]
    whole = blocks.reshape(*(lax.axis_size(a) for a in axes), *inside)
    for k in turns:
        whole = lax.all_to_all(whole, axes[k], k, k, tiled=True)
    return whole.reshape(-1, *inside)


def exchange_by_chip(value, groups, turns, split_dim, concat_dim):
    devices = lax.axis_size(groups[0]) * lax.axis_size(groups[1])
    blocks = cut_along(value, split_dim, devices)
    return laid_out(turned_blocks(blocks, groups, turns), concat_dim)


def sent_and_summed(value, axis, dim):
    blocks = cut_along(value, dim, lax.axis_size(axis))
    arrived = lax.all_to_all(blocks, axis, split_axis=0, concat_axis=0, tiled=True)
    return arrived.astype(jnp.float32).sum(axis=0)


def rms_norm(tokens, norm_gain):
    widened = tokens.astype(jnp.float32)
    scaled = widened * lax.rsqrt(jnp.mean(widened * widened, axis=-1, keepdims=True) + epsilon)
    return (scaled * norm_gain).astype(jnp.bfloat16)


def body(tokens, norm_gain, w_gate, w_up, w_down, expert_ids, gate_weights):
    tok_rows, model_width = tokens.shape
    top_count = expert_ids.shape[1]
    ep_count = lax.axis_size(EP)
    tp_count = lax.axis_size("tp")
    local_experts = w_gate.shape[0]
    experts_all = local_experts * ep_count
    capacity = min(tok_rows, tok_rows * top_count * 4 // (3 * experts_all))
    normed = rms_norm(tokens, norm_gain)
    flat_ids = expert_ids.reshape(-1)
    onehot = (flat_ids[:, None] == jnp.arange(experts_all, dtype=jnp.int32)[None, :]).astype(
        jnp.int32
    )
    before = jnp.cumsum(onehot, axis=0) - onehot
    slot_index = jnp.sum(before * onehot, axis=1)
    dest_row = flat_ids * capacity + slot_index
    owner_tok = jnp.arange(tok_rows * top_count, dtype=jnp.int32) // top_count
    slot_table = (
        jnp.full((experts_all * capacity,), tok_rows, jnp.int32).at[dest_row].set(owner_tok)
    )
    padded = jnp.concatenate([normed, jnp.zeros((1, model_width), jnp.bfloat16)], axis=0)
    send_buffer = padded[slot_table].reshape(experts_all, capacity, model_width)
    col_share = model_width // tp_count
    col_part = lax.dynamic_slice_in_dim(send_buffer, lax.axis_index("tp") * col_share, col_share, 2)
    received = exchange_by_chip(col_part, ("ep_0", "ep_1"), (1, 0), 0, 0)
    received = lax.all_gather(received, "tp", axis=2, tiled=True)
    expert_rows = received.reshape(ep_count, local_experts, capacity, model_width)
    gate_pre = jnp.einsum("sjcd,jdf->sjcf", expert_rows, w_gate, preferred_element_type=jnp.float32)
    up_pre = jnp.einsum("sjcd,jdf->sjcf", expert_rows, w_up, preferred_element_type=jnp.float32)
    gated = jnp.minimum(gate_pre, clamp_limit)
    linear = jnp.clip(up_pre, -clamp_limit, clamp_limit)
    activated = (gated * jax.nn.sigmoid(swish_alpha * gated) * (linear + 1.0)).astype(jnp.bfloat16)
    partial_value = jnp.einsum(
        "sjcf,jfd->sjcd", activated, w_down, preferred_element_type=jnp.float32
    ).astype(jnp.bfloat16)
    summed = sent_and_summed(partial_value, "tp", 3).astype(jnp.bfloat16)
    returned = exchange_by_chip(summed, ("ep_0", "ep_1"), (1, 0), 0, 0)
    returned = returned.reshape(experts_all * capacity, returned.shape[3])
    picked = returned[dest_row].reshape(tok_rows, top_count, returned.shape[1]).astype(jnp.float32)
    return jnp.sum(picked * gate_weights[:, :, None], axis=1).astype(jnp.bfloat16)


def solution(mesh):
    torus = Mesh(
        mesh.devices.reshape(mesh.shape["grp"], 32, 2, mesh.shape["tp"]),
        ("grp", "ep_0", "ep_1", "tp"),
    )
    return jax.shard_map(
        body,
        mesh=torus,
        in_specs=(
            P(GRP_EP, None),
            P(),
            P(EP, None, "tp"),
            P(EP, None, "tp"),
            P(EP, "tp", None),
            P(GRP_EP, None),
            P(GRP_EP, None),
        ),
        out_specs=P(GRP_EP, "tp"),
        check_vma=False,
    )
```

profile of v0, /device:TPU:33, one launch (start us, length us, event | category | flops | bytes accessed | tf_op | source)
XLA Modules:
  0.0 449.6 jit_solution(9208010235505050856)
XLA Ops:
  6.6 0.9 copy.23
  7.4 0.1 eq.29
  7.6 0.1 eq.25
  7.7 0.7 broadcast_multiply_fusion
  8.4 1.8 reduce-window.6
  10.2 0.3 slice_reduce_fusion
  10.5 0.1 copy.22
  10.6 0.1 mul.68
  10.7 0.1 fusion.26
  10.9 3.4 scatter_custom_fusion
  14.3 1.4 fusion
  15.7 1.4 fusion.2
  17.1 0.1 concatenate.3
  17.2 6.0 %gather_fusion = bf16[1024,2048]{1,0:T(8,128)(2,1)} fusion(bf16[193,2048]{1,0:T(8,128)(2,1)S(1)} %concatenate.3, s32[1024]{0:T(1024)S(1)} %fusion.30), kind=kCustom, calls=%fused_computation | custom fusion | bytes 8392704 | tf_op jit(solution)/shard_map/gather | solution.py:74
  23.2 1.3 constant_dynamic-slice_fusion
  24.6 45.8 %all_to_all.25 = bf16[32,2,1,16,512]{4,3,0,2,1:T(8,128)(2,1)S(1)} all-to-all(bf16[32,2,1,16,512]{4,3,0,2,1:T(8,128)(2,1)S(1)} %copy.26), channel_id=1, replica_groups=mesh['grp'=2,'ep_0'=32,'ep_1'=2,'tp'=4] {'ep_1'}, dimensions={1} | all-to-all | bytes 2097152 | tf_op jit(solution)/shard_map/all_to_all | solution.py:31
  70.4 0.1 copy.27
  70.5 110.0 %all_to_all.26 = bf16[32,2,1,16,512]{4,3,1,2,0:T(8,128)(2,1)} all-to-all(bf16[32,2,1,16,512]{4,3,1,2,0:T(8,128)(2,1)S(1)} %copy.27), channel_id=1, replica_groups=mesh['grp'=2,'ep_0'=32,'ep_1'=2,'tp'=4] {'ep_0'}, dimensions={0} | all-to-all | bytes 2097152 | tf_op jit(solution)/shard_map/all_to_all | solution.py:31
  180.5 51.5 %all-gather.2.cloned.1.call-done = bf16[64,16,2048]{2,1,0:T(8,128)(2,1)} async-done(((bf16[64,16,512]{2,1,0:T(8,128)(2,1)}), bf16[64,16,2048]{2,1,0:T(8,128)(2,1)}) %all-gather.2.cloned.1.call-update) | async-done | bytes 4194320 | tf_op jit(solution)/shard_map/all_gather | solution.py:78
  232.1 4.5 %fusion.3 = f32[64,1,16,256]{3,2,0,1:T(8,128)} fusion(bf16[64,16,2048]{2,1,0:T(8,128)(2,1)} %all-gather.2.cloned.1.call-done, bf16[1,2048,256]{2,1,0:T(8,128)(2,1)S(1)} %copy-done.2), kind=kOutput, calls=%fused_computation.12 | convolution fusion | flops 1074003968 | bytes 6291456 | tf_op jit(solution)/shard_map/sjcd,jdf->sjcf/dot_general | solution.py:80
  236.6 8.9 %convolution_convert_fusion = bf16[64,16,2048]{2,1,0:T(8,128)(2,1)} fusion(bf16[64,16,2048]{2,1,0:T(8,128)(2,1)} %all-gather.2.cloned.1.call-done, bf16[1,256,2048]{2,1,0:T(8,128)(2,1)S(1)} %copy-done, bf16[1,2048,256]{2,1,0:T(8,128)(2,1)S(1)} %copy-done.3, f32[64,1,16,256]{3,2,0,1:T(8,128)} %fusion.3), kind=kOutput, calls=%fused_computation.4 | convolution fusion | flops 2151940096 | bytes 11534336 | tf_op jit(solution)/shard_map/sjcf,jfd->sjcd/dot_general | solution.py:85
  245.4 2.8 copy.36
  248.3 51.3 %all_to_all.27 = bf16[4,64,1,16,512]{4,3,1,2,0:T(8,128)(2,1)} all-to-all(bf16[4,64,1,16,512]{4,3,1,2,0:T(8,128)(2,1)S(1)} %bitcast.77), channel_id=1, replica_groups=mesh['grp'=2,'ep_0'=32,'ep_1'=2,'tp'=4] {'tp'}, dimensions={0} | all-to-all | bytes 8388608 | tf_op jit(solution)/shard_map/all_to_all | solution.py:43
  299.6 3.3 reduce_sum.44
  303.0 6.1 %all_to_all.28 = bf16[32,2,1,1,16,512]{5,4,0,3,2,1:T(8,128)(2,1)S(1)} all-to-all(bf16[32,2,1,1,16,512]{5,4,0,3,2,1:T(8,128)(2,1)S(1)} %copy.29), channel_id=1, replica_groups=mesh['grp'=2,'ep_0'=32,'ep_1'=2,'tp'=4] {'ep_1'}, dimensions={1} | all-to-all | bytes 2097152 | tf_op jit(solution)/shard_map/all_to_all | solution.py:31
  309.1 1.1 copy.30
  310.2 23.4 %all-to-all-start.4 = ((bf16[32,2,1,1,16,512]{5,4,1,3,2,0:T(8,128)(2,1)}), bf16[32,2,1,1,16,512]{5,4,1,3,2,0:T(8,128)(2,1)S(1)}, u32[]{:S(2)}, u32[]{:S(2)}) async-start(bf16[32,2,1,1,16,512]{5,4,1,3,2,0:T(8,128)(2,1)} %copy.30), calls=%async_computation.4 | async-start | bytes 2097152 | tf_op jit(solution)/shard_map/all_to_all | solution.py:31
  333.6 0.1 copy.31
  333.7 104.2 %all-to-all-done.4 = bf16[32,2,1,1,16,512]{5,4,1,3,2,0:T(8,128)(2,1)S(1)} async-done(((bf16[32,2,1,1,16,512]{5,4,1,3,2,0:T(8,128)(2,1)}), bf16[32,2,1,1,16,512]{5,4,1,3,2,0:T(8,128)(2,1)S(1)}, u32[]{:S(2)}, u32[]{:S(2)}) %all-to-all-start.4) | async-done | bytes 1048608 | tf_op jit(solution)/shard_map/all_to_all | solution.py:31
  437.9 2.7 gather_fusion.1
  440.6 0.5 reshape.102
  441.1 1.7 multiply_reduce_fusion
  (19 shorter events, 0.3 us)
Async XLA Ops:
  6.5 230.0 %copy-start = (bf16[1,256,2048]{2,1,0:T(8,128)(2,1)S(1)}, bf16[1,256,2048]{2,1,0:T(8,128)(2,1)}, u32[]{:S(2)}) copy-start(bf16[1,256,2048]{2,1,0:T(8,128)(2,1)} %param.11) | copy-start | bytes 3145732
  6.6 225.5 %all-gather.2.cloned.1.call-start = ((), (), s32[]{:S(2)}) async-start(), calls=%async_computation.5 | async-start | bytes 5242880 | tf_op jit(solution)/shard_map/all_gather | solution.py:78
  24.6 207.5 %copy-start.2 = (bf16[1,2048,256]{2,1,0:T(8,128)(2,1)S(1)}, bf16[1,2048,256]{2,1,0:T(8,128)(2,1)}, u32[]{:S(2)}) copy-start(bf16[1,2048,256]{2,1,0:T(8,128)(2,1)} %param.9) | copy-start | bytes 3145732
  180.5 56.1 %copy-start.3 = (bf16[1,2048,256]{2,1,0:T(8,128)(2,1)S(1)}, bf16[1,2048,256]{2,1,0:T(8,128)(2,1)}, u32[]{:S(2)}) copy-start(bf16[1,2048,256]{2,1,0:T(8,128)(2,1)} %param.10) | copy-start | bytes 3145732
  302.9 30.7 %copy-start.1 = (f32[192,4]{0,1:T(4,128)S(1)}, f32[192,4]{0,1:T(4,128)}, u32[]{:S(2)}) copy-start(f32[192,4]{0,1:T(4,128)} %param.13) | copy-start | bytes 9220
  310.2 127.7 %all-to-all-start.4 = ((bf16[32,2,1,1,16,512]{5,4,1,3,2,0:T(8,128)(2,1)}), bf16[32,2,1,1,16,512]{5,4,1,3,2,0:T(8,128)(2,1)S(1)}, u32[]{:S(2)}, u32[]{:S(2)}) async-start(bf16[32,2,1,1,16,512]{5,4,1,3,2,0:T(8,128)(2,1)} %copy.30), calls=%async_computation.4 | async-start | bytes 2097152 | tf_op jit(solution)/shard_map/all_to_all | solution.py:31
Sparse Core Ops, SparseCore 0:
  180.7 51.3 all-gather.1
where the time goes:
time: 450 us
  blocking collectives  213 us (47%)
  waiting for transfers between devices  156 us (35%)
  starting transfers between devices  23.4 us (5%)
  local copies, waits for them, and re-layouts  19.8 us (4%)
  between operations  13.6 us (3%)
  matrix products  13.4 us (3%)
  other arithmetic  10.5 us (2%)
    all_to_all x3, blocking collectives, turned_blocks(): whole = lax.all_to_all(whole, axes[k], k, k, tiled=True)  162 us
    all_to_all x1, waiting for transfers between devices, turned_blocks(): whole = lax.all_to_all(whole, axes[k], k, k, tiled=True)  104 us
    all_gather x1, waiting for transfers between devices, body(): received = lax.all_gather(received, 'tp', axis=2, tiled=True)  51.5 us
    all_to_all x1, blocking collectives, sent_and_summed(): lax.all_to_all(blocks, axis, split_axis=0, concat_axis=0, tiled=True)  51.3 us
    all_to_all x1, starting transfers between devices, turned_blocks(): whole = lax.all_to_all(whole, axes[k], k, k, tiled=True)  23.4 us
  transfers between devices with their start and end apart: 2, of which 2 were waited for; matrix products, arithmetic and copies ran while one was open for 0% of the time, Pallas kernels for 0%

commit v1 on v0

v1 whole, which is shorter than its diff:
```python
import functools

import jax
import jax.numpy as jnp
from jax import lax
from jax.experimental import pallas as pl
from jax.experimental.pallas import tpu as pltpu
from jax.sharding import PartitionSpec as P

MESH = pl.DeviceIdType.MESH
BF16 = jnp.bfloat16
F32 = jnp.float32

epsilon = 1e-06
clamp_limit = 7.0
swish_alpha = 1.702

CORES = 2
PARTS = 3


def kernel(
    cfg,
    tok_ref,
    gain_ref,
    meta_ref,
    wg_hbm,
    wu_hbm,
    wd_hbm,
    out_ref,
    ag,
    agm,
    rs,
    rsend,
    grow,
    stg,
    part,
    relay,
    direct,
    pair,
    pair_in,
    y_own,
    y_out,
    y_sib,
    cbuf,
    back,
    wg,
    wu,
    wd,
    w_sem,
    ag_send,
    ag_recv,
    rs_send,
    rs_recv,
    sel_send,
    sel_recv,
    xg_send,
    xg_recv,
    xr_send,
    xr_recv,
    y_send,
    y_recv,
):
    nz, nx, cap, rows, cols, pad = cfg
    half = nz // 2
    sub = rows // PARTS
    ep = lax.axis_index("ep")
    x = lax.axis_index("tp")
    z, c = ep // CORES, ep % CORES
    f = 1 - 2 * c

    def wrap(v, n):
        return lax.rem(v + 2 * n, n)

    z_to = (
        {"ep": wrap(z + 1, nz) * CORES + c},
        {"ep": wrap(z - 1, nz) * CORES + c},
    )
    sib = {"ep": z * CORES + 1 - c}
    x_up, x_dn = {"tp": wrap(x + 1, nx)}, {"tp": wrap(x - 1, nx)}
    x_f, x_b = wrap(x + f, nx), wrap(x - f, nx)
    x_far = wrap(x + 2, nx)

    def reach(d):
        return half - jnp.where(c == d, 0, 1)

    def hops(d, j):
        if j == PARTS:
            return reach(d)
        return reach(d) - (sub * j) // (CORES * cap)

    def remote(src, dst, ssem, rsem, dev):
        return pltpu.make_async_remote_copy(
            src_ref=src, dst_ref=dst, send_sem=ssem, recv_sem=rsem,
            device_id=dev, device_id_type=MESH,
        )

    def ag_copy(d, h, j):
        ssem = ag_send.at[d, lax.rem(h, 2), j]
        if j == PARTS:
            return remote(agm.at[d, h], agm.at[d, h + 1], ssem, ag_recv.at[d, h + 1, j], z_to[d])
        win = pl.ds(j * sub, sub)
        return remote(
            ag.at[d, h, win], ag.at[d, h + 1, win], ssem, ag_recv.at[d, h + 1, j], z_to[d]
        )

    def rs_copy(d, h, j):
        win = pl.ds(j * sub, sub)
        par = lax.rem(h, 2)
        return remote(
            rsend.at[d, par, win], rs.at[d, h - 1, win],
            rs_send.at[d, par, j], rs_recv.at[d, h - 1, j], z_to[1 - d],
        )

    def sel_copy(h):
        return remote(
            stg.at[h], grow.at[x, h, pl.ds(2 * cap, 2 * cap)], sel_send.at[h], sel_recv.at[h], sib
        )

    def xg_copy(h, way):
        if way == 0:
            return remote(grow.at[x, h], grow.at[x, h], xg_send.at[h, 0], xg_recv.at[h, 0], x_up)
        if way == 1:
            return remote(grow.at[x, h], grow.at[x, h], xg_send.at[h, 1], xg_recv.at[h, 1], x_dn)
        return remote(
            grow.at[x_b, h], grow.at[x_b, h], xg_send.at[h, 2], xg_recv.at[h, 2], {"tp": x_f}
        )

    def xr_copy(h, way):
        if way == 0:
            return remote(
                part.at[h, x_far], relay.at[h], xr_send.at[h, 0], xr_recv.at[h, 0], {"tp": x_f}
            )
        if way == 1:
            return remote(
                part.at[h, x_b], direct.at[h], xr_send.at[h, 1], xr_recv.at[h, 1], {"tp": x_b}
            )
        return remote(
            pair.at[h], pair_in.at[h], xr_send.at[h, 2], xr_recv.at[h, 2], {"tp": x_f}
        )

    def y_copy(h):
        return remote(y_out.at[h], y_sib.at[h], y_send.at[h], y_recv.at[h], sib)

    weights = [
        pltpu.make_async_copy(src.at[0], dst, w_sem.at[k])
        for k, (src, dst) in enumerate(((wg_hbm, wg), (wu_hbm, wu), (wd_hbm, wd)))
    ]
    for copy in weights:
        copy.start()

    for d in range(2):
        for j in range(PARTS + 1):
            low = half - 1 - (0 if j == PARTS else (sub * j) // (CORES * cap))
            for h in range(max(low, 0), half + 1):
                if j < PARTS:
                    @pl.when(h >= hops(d, j))
                    def _():
                        rs[d, h, pl.ds(j * sub, sub)] = jnp.zeros((sub, cols), BF16)
                if h >= 1:
                    @pl.when(h > hops(d, j))
                    def _():
                        if j < PARTS:
                            ag[d, h, pl.ds(j * sub, sub)] = jnp.zeros((sub, cols), BF16)
                        else:
                            agm[d, h] = jnp.full((8, pad), -1.0, F32)

    barrier = pltpu.get_barrier_semaphore()
    for dev in (*z_to, sib, x_up, x_dn):
        pl.semaphore_signal(barrier, inc=1, device_id=dev, device_id_type=MESH)

    widened = tok_ref[...].astype(F32)
    scale = lax.rsqrt(jnp.mean(widened * widened, axis=-1, keepdims=True) + epsilon)
    mine = pl.ds(pl.multiple_of(x * cols, cols), cols)
    own_cols = tok_ref[:, mine].astype(F32) * scale
    own_cols = (own_cols * gain_ref[:, mine]).astype(BF16)

    meta = meta_ref[...]
    ids = meta[0:4].astype(jnp.int32)
    ahead = lax.shift_right_arithmetic(ids, 1) - z
    ahead = jnp.where(ahead < 0, ahead + nz, ahead)
    behind = jnp.where(ahead == 0, 0, nz - ahead)
    lane = lax.broadcasted_iota(jnp.int32, (pad, pad), 1)
    line = lax.broadcasted_iota(jnp.int32, (pad, pad), 0)
    for d, dist in enumerate((ahead, behind)):
        far = jnp.max(jnp.where(dist <= reach(d), dist, 0), axis=0, keepdims=True)
        far = jnp.where(lane[0:1] < rows, far, -1).astype(F32)
        by_lane = jnp.broadcast_to(far, (pad, pad))
        by_line = by_lane.T
        first = (by_line > by_lane) | ((by_line == by_lane) & (line < lane))
        rank_lane = jnp.sum(jnp.where(first, 1.0, 0.0), axis=0, keepdims=True)
        later = (by_lane > by_line) | ((by_lane == by_line) & (lane < line))
        rank_line = jnp.sum(jnp.where(later, 1.0, 0.0), axis=1, keepdims=True)
        order = jnp.where(rank_lane == line.astype(F32), 1.0, 0.0).astype(BF16)
        back_to = jnp.where(rank_line == lane.astype(F32), 1.0, 0.0).astype(BF16)
        ag[d, 0] = jnp.dot(
            order[:rows, :rows], own_cols, preferred_element_type=F32
        ).astype(BF16)
        agm[d, 0] = jnp.dot(meta.astype(BF16), back_to, preferred_element_type=F32)
        back[d] = back_to

    pl.semaphore_wait(barrier, 5)

    sub_line = lax.broadcasted_iota(jnp.int32, (2 * cap, pad), 0)
    own_slot = jnp.where(sub_line < cap, sub_line, sub_line - cap).astype(F32)

    def select(d, h):
        valid = h <= reach(d)
        if d == 1:
            valid = valid & (h >= 1)
        expert = jnp.where(sub_line < cap, ep, z * CORES + 1 - c)
        expert = jnp.where(valid, expert, -7).astype(F32)
        meta = agm[d, h]
        named = jnp.zeros((2 * cap, pad), F32)
        weight = jnp.zeros((2 * cap, pad), F32)
        for k in range(4):
            same = jnp.where(meta[k : k + 1] == expert, 1.0, 0.0)
            named = named + same
            weight = weight + same * meta[k + 4 : k + 5]
        before = jnp.where(
            lax.broadcasted_iota(jnp.int32, (pad, pad), 0)
            < lax.broadcasted_iota(jnp.int32, (pad, pad), 1),
            1.0, 0.0,
        ).astype(BF16)
        slot = jnp.dot(named.astype(BF16), before, preferred_element_type=F32)
        pick = jnp.where(slot == own_slot, named, 0.0)
        spread = (pick * weight).astype(BF16)
        eye = jnp.where(
            lax.broadcasted_iota(jnp.int32, (rows, pad), 0)
            == lax.broadcasted_iota(jnp.int32, (rows, pad), 1),
            1.0, 0.0,
        ).astype(BF16)
        cbuf[d, h] = lax.dot_general(
            eye, spread, (((1,), (1,)), ((), ())), preferred_element_type=F32
        ).astype(BF16)
        got = jnp.dot(
            pick.astype(BF16)[:, :rows], ag[d, h], preferred_element_type=F32
        ).astype(BF16)
        grow[x, h, pl.ds(d * cap, cap)] = got[:cap]
        stg[h, pl.ds(d * cap, cap)] = got[cap:]

    def dispatch(i, _):
        @pl.when(i <= half)
        def _():
            for j in (PARTS, *range(PARTS)):
                for d in range(2):
                    @pl.when((i >= 1) & (i <= hops(d, j)))
                    def _():
                        ag_copy(d, i - 1, j).wait_recv()

                    @pl.when(i < hops(d, j))
                    def _():
                        @pl.when(i >= 2)
                        def _():
                            ag_copy(d, i - 2, j).wait_send()

                        ag_copy(d, i, j).start()

        @pl.when(i >= 2)
        def _():
            h = i - 2
            remote(
                grow.at[x_b, h], grow.at[x_b, h], xg_send.at[h, 2], xg_recv.at[h, c], x_up
            ).wait_recv()
            xg_copy(h, 2).start()

        @pl.when((i >= 1) & (i <= half + 1))
        def _():
            h = i - 1
            sel_copy(h).wait_recv()
            xg_copy(h, 0).start()
            xg_copy(h, 1).start()

        @pl.when(i <= half)
        def _():
            select(0, i)
            select(1, i)
            sel_copy(i).start()

        return 0

    lax.fori_loop(0, half + 3, dispatch, 0)

    for copy in weights:
        copy.wait()

    def blend(d, h, j):
        win = pl.ds(j * sub, sub)
        mid = pl.ds(d * cap, cap)
        both = jnp.concatenate([y_own[h, mid], y_sib[h, mid]], axis=0)
        gain = jnp.dot(cbuf[d, h, win], both, preferred_element_type=F32)
        return rs[d, h, win].astype(F32) + gain

    def gather_back(i, _):
        @pl.when(i >= 3)
        def _():
            h = half - i + 3
            y_copy(h).wait_recv()
            for j in range(PARTS):
                for d in range(2):
                    @pl.when(h + 1 <= hops(d, j))
                    def _():
                        rs_copy(d, h + 1, j).wait_recv()

                    @pl.when(h + 2 <= hops(d, j))
                    def _():
                        rs_copy(d, h + 2, j).wait_send()

                    @pl.when(h <= hops(d, j))
                    def _():
                        rsend[d, lax.rem(h, 2), pl.ds(j * sub, sub)] = blend(d, h, j).astype(BF16)
                        rs_copy(d, h, j).start()

        @pl.when((i >= 2) & (i <= half + 2))
        def _():
            h = half - i + 2
            xr_copy(h, 1).wait_recv()
            xr_copy(h, 2).wait_recv()
            total = (
                part[h, x].astype(F32) + direct[h].astype(F32) + pair_in[h].astype(F32)
            ).astype(BF16)
            y_own[h] = total[: 2 * cap]
            y_out[h] = total[2 * cap :]
            y_copy(h).start()

        @pl.when((i >= 1) & (i <= half + 1))
        def _():
            h = half - i + 1
            xr_copy(h, 0).wait_recv()
            pair[h] = (part[h, x_f].astype(F32) + relay[h].astype(F32)).astype(BF16)
            xr_copy(h, 2).start()

        @pl.when(i <= half)
        def _():
            h = half - i
            remote(
                grow.at[x_f, h], grow.at[x_f, h], xg_send.at[h, 2], xg_recv.at[h, 1 - c], x_up
            ).wait_recv()
            xg_copy(h, 2).wait_recv()
            gate = jnp.zeros((4 * cap, wg.shape[1]), F32)
            up = jnp.zeros((4 * cap, wg.shape[1]), F32)
            for k in range(nx):
                block = grow[k, h]
                gate = gate + jnp.dot(
                    block, wg[pl.ds(k * cols, cols)], preferred_element_type=F32
                )
                up = up + jnp.dot(block, wu[pl.ds(k * cols, cols)], preferred_element_type=F32)
            gated = jnp.minimum(gate, clamp_limit)
            linear = jnp.clip(up, -clamp_limit, clamp_limit)
            active = (gated * jax.nn.sigmoid(swish_alpha * gated) * (linear + 1.0)).astype(BF16)
            for k in range(nx):
                part[h, k] = jnp.dot(
                    active, wd[:, pl.ds(k * cols, cols)], preferred_element_type=F32
                ).astype(BF16)
            xr_copy(h, 0).start()
            xr_copy(h, 1).start()

        return 0

    lax.fori_loop(0, half + 3, gather_back, 0)

    y_copy(0).wait_recv()
    total = jnp.zeros((rows, cols), F32)
    for d in range(2):
        for j in range(PARTS):
            @pl.when(1 <= hops(d, j))
            def _():
                rs_copy(d, 1, j).wait_recv()
        held = jnp.concatenate(
            [blend(d, 0, j).astype(BF16) for j in range(PARTS)], axis=0
        )
        total = total + jnp.dot(back[d, :rows, :rows], held, preferred_element_type=F32)
    out_ref[...] = total.astype(BF16)

    for d in range(2):
        for j in range(PARTS + 1):
            for k in (1, 2):
                @pl.when(hops(d, j) >= k)
                def _():
                    ag_copy(d, hops(d, j) - k, j).wait_send()
                if j < PARTS:
                    @pl.when(hops(d, j) >= k)
                    def _():
                        rs_copy(d, k, j).wait_send()

    def drain(h, _):
        sel_copy(h).wait_send()
        y_copy(h).wait_send()
        for way in range(3):
            xg_copy(h, way).wait_send()
            xr_copy(h, way).wait_send()
        return 0

    lax.fori_loop(0, half + 1, drain, 0)


def body(ep_count, tp_count, tokens, norm_gain, w_gate, w_up, w_down, expert_ids, gate_weights):
    rows, width = tokens.shape
    top = expert_ids.shape[1]
    experts = w_gate.shape[0] * ep_count
    cap = min(rows, rows * top * 4 // (3 * experts))
    cols = width // tp_count
    hidden = w_gate.shape[2]
    pad = -(-rows // 128) * 128
    steps = ep_count // CORES // 2 + 1
    meta = jnp.concatenate([expert_ids.astype(F32).T, gate_weights.T], axis=0)
    meta = jnp.pad(meta, ((0, 0), (0, pad - rows)), constant_values=-1.0)
    vmem = pl.BlockSpec(memory_space=pltpu.VMEM)
    hbm = pl.BlockSpec(memory_space=pl.ANY)
    dma = pltpu.SemaphoreType.DMA
    block = (4 * cap, cols)
    return pl.pallas_call(
        functools.partial(kernel, (ep_count // CORES, tp_count, cap, rows, cols, pad)),
        out_shape=jax.ShapeDtypeStruct((rows, cols), BF16),
        in_specs=[vmem, vmem, vmem, hbm, hbm, hbm],
        out_specs=vmem,
        scratch_shapes=[
            pltpu.VMEM((2, steps, rows, cols), BF16),
            pltpu.VMEM((2, steps, 8, pad), F32),
            pltpu.VMEM((2, steps, rows, cols), BF16),
            pltpu.VMEM((2, 2, rows, cols), BF16),
            pltpu.VMEM((tp_count, steps, *block), BF16),
            pltpu.VMEM((steps, 2 * cap, cols), BF16),
            pltpu.VMEM((steps, tp_count, *block), BF16),
            pltpu.VMEM((steps, *block), BF16),
            pltpu.VMEM((steps, *block), BF16),
            pltpu.VMEM((steps, *block), BF16),
            pltpu.VMEM((steps, *block), BF16),
            pltpu.VMEM((steps, 2 * cap, cols), BF16),
            pltpu.VMEM((steps, 2 * cap, cols), BF16),
            pltpu.VMEM((steps, 2 * cap, cols), BF16),
            pltpu.VMEM((2, steps, rows, 2 * cap), BF16),
            pltpu.VMEM((2, pad, pad), BF16),
            pltpu.VMEM((width, hidden), BF16),
            pltpu.VMEM((width, hidden), BF16),
            pltpu.VMEM((hidden, width), BF16),
            dma((3,)),
            dma((2, 2, PARTS + 1)),
            dma((2, steps, PARTS + 1)),
            dma((2, 2, PARTS)),
            dma((2, steps, PARTS)),
            dma((steps,)),
            dma((steps,)),
            dma((steps, 3)),
            dma((steps, 3)),
            dma((steps, 3)),
            dma((steps, 3)),
            dma((steps,)),
            dma((steps,)),
        ],
        compiler_params=pltpu.CompilerParams(
            collective_id=0, has_side_effects=True, vmem_limit_bytes=60 * 1024 * 1024
        ),
    )(tokens, norm_gain.reshape(1, width), meta, w_gate, w_up, w_down)


def solution(mesh):
    return jax.shard_map(
        functools.partial(body, mesh.shape["ep"], mesh.shape["tp"]),
        mesh=mesh,
        in_specs=(
            P(("grp", "ep"), None),
            P(),
            P("ep", None, "tp"),
            P("ep", None, "tp"),
            P("ep", "tp", None),
            P(("grp", "ep"), None),
            P(("grp", "ep"), None),
        ),
        out_specs=P(("grp", "ep"), "tp"),
        check_vma=False,
    )
```

time: 450 us -> 229 us (0.51)
  Pallas kernels: 0 us -> 226 us
  blocking collectives: 213 us -> 0 us
  waiting for transfers between devices: 156 us -> 0 us
  starting transfers between devices: 23.4 us -> 0 us
  local copies, waits for them, and re-layouts: 19.8 us -> 1.62 us
  between operations: 13.6 us -> 0.01 us
  matrix products: 13.4 us -> 0 us
  other arithmetic: 10.5 us -> 1.31 us
    pallas_call x0 -> x1, Pallas kernels: none -> 226 us  [body(): pl.pallas_call(functools.partial(kernel, (ep_count // CORES, tp_count, ca...]
    all_to_all x4 -> x0, blocking collectives: 213 us -> none  [the longest x3 162 us: turned_blocks(): whole = lax.all_to_all(whole, axes[k], k, k, tiled=True)]
    all_to_all x1 -> x0, waiting for transfers between devices: 104 us -> none  [turned_blocks(): whole = lax.all_to_all(whole, axes[k], k, k, tiled=True)]
    all_gather x1 -> x0, waiting for transfers between devices: 51.5 us -> none  [body(): received = lax.all_gather(received, 'tp', axis=2, tiled=True)]
    all_to_all x1 -> x0, starting transfers between devices: 23.4 us -> none  [turned_blocks(): whole = lax.all_to_all(whole, axes[k], k, k, tiled=True)]
    dot_general x2 -> x0, matrix products: 13.4 us -> none  [the longest x1 8.85 us: body(): jnp.einsum('sjcf,jfd->sjcd', activated, w_down, preferred_element_type=jn...]
    gather x2 -> x0, local copies, waits for them, and re-layouts: 8.69 us -> none  [the longest x1 6.02 us: body(): send_buffer = padded[slot_table].reshape(experts_all, capacity, model_width)]
    reduce_sum x4 -> x0, other arithmetic: 6.53 us -> none  [the longest x1 3.33 us: sent_and_summed(): return arrived.astype(jnp.float32).sum(axis=0)]
  transfers between devices with their start and end apart: 2 -> 0, of which waited for: 2 -> 0; matrix products, arithmetic and copies ran while one was open for 0% -> 0% of each run, Pallas kernels for 0% -> 0%
where the time goes in v1:
time: 229 us
  Pallas kernels  226 us (99%)
    pallas_call x1, Pallas kernels, body(): pl.pallas_call(functools.partial(kernel, (ep_count // CORES, tp_count, ca...  226 us

profile of v1, /device:TPU:33, one launch (start us, length us, event | category | flops | bytes accessed | tf_op | source)
XLA Modules:
  0.0 228.5 jit_solution(10726062583224713326)
XLA Ops:
  0.0 0.0 copy-start
  0.0 0.7 convert_bitcast_fusion
  0.7 0.0 copy-done
  0.7 0.6 select_maximum_fusion.meta_ref
  1.3 225.6 %shard_map.73 = bf16[192,512]{1,0:T(8,128)(2,1)} custom-call(bf16[192,2048]{1,0:T(8,128)(2,1)} %tok_ref.1, f32[1,2048]{1,0:T(1,128)} %bitcast.4, f32[8,256]{1,0:T(8,128)} %select_maximum_fusion.meta_ref, bf16[1,2048,256]{2,1,0:T(8,128)(2,1)} %wg_hbm.1, bf16[1,2048,256]{2,1,0:T(8,128)(2,1)} %wu_hbm.1, bf16[1,256,2048]{2,1,0:T(8,128)(2,1)} %wd_hbm.1), custom_call_target="tpu_custom_call" | custom-call | tf_op jit(solution)/shard_map/pallas_call | solution.py:412
  226.9 1.6 copy.9
Async XLA Ops:
  0.0 0.7 copy-start

commit v2 on v1

--- a/solution.py
+++ b/solution.py
@@ -16,12 +16,12 @@
 swish_alpha = 1.702
 
 CORES = 2
-PARTS = 3
+PARTS = 6
 
 
 def kernel(
     cfg,
-    tok_ref,
+    tok_hbm,
     gain_ref,
     meta_ref,
     wg_hbm,
@@ -43,7 +43,9 @@
     y_out,
     y_sib,
     cbuf,
+    gains,
     back,
+    tok,
     wg,
     wu,
     wd,
@@ -142,6 +144,12 @@
     def y_copy(h):
         return remote(y_out.at[h], y_sib.at[h], y_send.at[h], y_recv.at[h], sib)
 
+    barrier = pltpu.get_barrier_semaphore()
+    for dev in (*z_to, sib, x_up, x_dn):
+        pl.semaphore_signal(barrier, inc=1, device_id=dev, device_id_type=MESH)
+
+    load = pltpu.make_async_copy(tok_hbm, tok, w_sem.at[3])
+    load.start()
     weights = [
         pltpu.make_async_copy(src.at[0], dst, w_sem.at[k])
         for k, (src, dst) in enumerate(((wg_hbm, wg), (wu_hbm, wu), (wd_hbm, wd)))
@@ -165,14 +173,11 @@
                         else:
                             agm[d, h] = jnp.full((8, pad), -1.0, F32)
 
-    barrier = pltpu.get_barrier_semaphore()
-    for dev in (*z_to, sib, x_up, x_dn):
-        pl.semaphore_signal(barrier, inc=1, device_id=dev, device_id_type=MESH)
-
-    widened = tok_ref[...].astype(F32)
+    load.wait()
+    widened = tok[...].astype(F32)
     scale = lax.rsqrt(jnp.mean(widened * widened, axis=-1, keepdims=True) + epsilon)
     mine = pl.ds(pl.multiple_of(x * cols, cols), cols)
-    own_cols = tok_ref[:, mine].astype(F32) * scale
+    own_cols = tok[:, mine].astype(F32) * scale
     own_cols = (own_cols * gain_ref[:, mine]).astype(BF16)
 
     meta = meta_ref[...]
@@ -256,6 +261,19 @@
 
                         ag_copy(d, i, j).start()
 
+        @pl.when((i >= 1) & (i <= half + 1))
+        def _():
+            h = i - 1
+            sel_copy(h).wait_recv()
+            xg_copy(h, 0).start()
+            xg_copy(h, 1).start()
+
+        @pl.when(i <= half)
+        def _():
+            select(0, i)
+            select(1, i)
+            sel_copy(i).start()
+
         @pl.when(i >= 2)
         def _():
             h = i - 2
@@ -264,19 +282,6 @@
             ).wait_recv()
             xg_copy(h, 2).start()
 
-        @pl.when((i >= 1) & (i <= half + 1))
-        def _():
-            h = i - 1
-            sel_copy(h).wait_recv()
-            xg_copy(h, 0).start()
-            xg_copy(h, 1).start()
-
-        @pl.when(i <= half)
-        def _():
-            select(0, i)
-            select(1, i)
-            sel_copy(i).start()
-
         return 0
 
     lax.fori_loop(0, half + 3, dispatch, 0)
@@ -284,18 +289,22 @@
     for copy in weights:
         copy.wait()
 
+    def spread_out(h):
+        for d in range(2):
+            mid = pl.ds(d * cap, cap)
+            both = jnp.concatenate([y_own[h, mid], y_sib[h, mid]], axis=0)
+            gains[d] = jnp.dot(cbuf[d, h], both, preferred_element_type=F32)
+
     def blend(d, h, j):
         win = pl.ds(j * sub, sub)
-        mid = pl.ds(d * cap, cap)
-        both = jnp.concatenate([y_own[h, mid], y_sib[h, mid]], axis=0)
-        gain = jnp.dot(cbuf[d, h, win], both, preferred_element_type=F32)
-        return rs[d, h, win].astype(F32) + gain
+        return rs[d, h, win].astype(F32) + gains[d, win]
 
     def gather_back(i, _):
         @pl.when(i >= 3)
         def _():
             h = half - i + 3
             y_copy(h).wait_recv()
+            spread_out(h)
             for j in range(PARTS):
                 for d in range(2):
                     @pl.when(h + 1 <= hops(d, j))
@@ -310,25 +319,6 @@
                     def _():
                         rsend[d, lax.rem(h, 2), pl.ds(j * sub, sub)] = blend(d, h, j).astype(BF16)
                         rs_copy(d, h, j).start()
-
-        @pl.when((i >= 2) & (i <= half + 2))
-        def _():
-            h = half - i + 2
-            xr_copy(h, 1).wait_recv()
-            xr_copy(h, 2).wait_recv()
-            total = (
-                part[h, x].astype(F32) + direct[h].astype(F32) + pair_in[h].astype(F32)
-            ).astype(BF16)
-            y_own[h] = total[: 2 * cap]
-            y_out[h] = total[2 * cap :]
-            y_copy(h).start()
-
-        @pl.when((i >= 1) & (i <= half + 1))
-        def _():
-            h = half - i + 1
-            xr_copy(h, 0).wait_recv()
-            pair[h] = (part[h, x_f].astype(F32) + relay[h].astype(F32)).astype(BF16)
-            xr_copy(h, 2).start()
 
         @pl.when(i <= half)
         def _():
@@ -355,11 +345,31 @@
             xr_copy(h, 0).start()
             xr_copy(h, 1).start()
 
+        @pl.when((i >= 1) & (i <= half + 1))
+        def _():
+            h = half - i + 1
+            xr_copy(h, 0).wait_recv()
+            pair[h] = (part[h, x_f].astype(F32) + relay[h].astype(F32)).astype(BF16)
+            xr_copy(h, 2).start()
+
+        @pl.when((i >= 2) & (i <= half + 2))
+        def _():
+            h = half - i + 2
+            xr_copy(h, 1).wait_recv()
+            xr_copy(h, 2).wait_recv()
+            total = (
+                part[h, x].astype(F32) + direct[h].astype(F32) + pair_in[h].astype(F32)
+            ).astype(BF16)
+            y_own[h] = total[: 2 * cap]
+            y_out[h] = total[2 * cap :]
+            y_copy(h).start()
+
         return 0
 
     lax.fori_loop(0, half + 3, gather_back, 0)
 
     y_copy(0).wait_recv()
+    spread_out(0)
     total = jnp.zeros((rows, cols), F32)
     for d in range(2):
         for j in range(PARTS):
@@ -412,7 +422,7 @@
     return pl.pallas_call(
         functools.partial(kernel, (ep_count // CORES, tp_count, cap, rows, cols, pad)),
         out_shape=jax.ShapeDtypeStruct((rows, cols), BF16),
-        in_specs=[vmem, vmem, vmem, hbm, hbm, hbm],
+        in_specs=[hbm, vmem, vmem, hbm, hbm, hbm],
         out_specs=vmem,
         scratch_shapes=[
             pltpu.VMEM((2, steps, rows, cols), BF16),
@@ -430,11 +440,13 @@
             pltpu.VMEM((steps, 2 * cap, cols), BF16),
             pltpu.VMEM((steps, 2 * cap, cols), BF16),
             pltpu.VMEM((2, steps, rows, 2 * cap), BF16),
+            pltpu.VMEM((2, rows, cols), F32),
             pltpu.VMEM((2, pad, pad), BF16),
+            pltpu.VMEM((rows, width), BF16),
             pltpu.VMEM((width, hidden), BF16),
             pltpu.VMEM((width, hidden), BF16),
             pltpu.VMEM((hidden, width), BF16),
-            dma((3,)),
+            dma((4,)),
             dma((2, 2, PARTS + 1)),
             dma((2, steps, PARTS + 1)),
             dma((2, 2, PARTS)),

time: 229 us -> 210 us (0.917)
  Pallas kernels: 226 us -> 207 us
    pallas_call x1, Pallas kernels: 226 us -> 207 us  [body(): pl.pallas_call(functools.partial(kernel, (ep_count // CORES, tp_count, ca...]
where the time goes in v2:
time: 210 us
  Pallas kernels  207 us (99%)
    pallas_call x1, Pallas kernels, body(): pl.pallas_call(functools.partial(kernel, (ep_count // CORES, tp_count, ca...  207 us

profile of v2, /device:TPU:33, one launch (start us, length us, event | category | flops | bytes accessed | tf_op | source)
XLA Modules:
  0.0 210.2 jit_solution(5516530502266274115)
XLA Ops:
  0.0 0.0 copy-start
  0.0 0.7 convert_bitcast_fusion
  0.7 0.0 copy-done
  0.7 0.6 select_maximum_fusion.meta_ref
  1.3 207.3 %shard_map.73 = bf16[192,512]{1,0:T(8,128)(2,1)} custom-call(bf16[192,2048]{1,0:T(8,128)(2,1)} %tok_hbm.1, f32[1,2048]{1,0:T(1,128)} %bitcast.4, f32[8,256]{1,0:T(8,128)} %select_maximum_fusion.meta_ref, bf16[1,2048,256]{2,1,0:T(8,128)(2,1)} %wg_hbm.1, bf16[1,2048,256]{2,1,0:T(8,128)(2,1)} %wu_hbm.1, bf16[1,256,2048]{2,1,0:T(8,128)(2,1)} %wd_hbm.1), custom_call_target="tpu_custom_call" | custom-call | tf_op jit(solution)/shard_map/pallas_call | solution.py:422
  208.6 1.6 copy.9
Async XLA Ops:
  0.0 0.7 copy-start

commit v3 on v2

--- a/solution.py
+++ b/solution.py
@@ -35,13 +35,8 @@
     grow,
     stg,
     part,
-    relay,
-    direct,
-    pair,
-    pair_in,
-    y_own,
-    y_out,
-    y_sib,
+    in_own,
+    in_sib,
     cbuf,
     gains,
     back,
@@ -54,14 +49,10 @@
     ag_recv,
     rs_send,
     rs_recv,
-    sel_send,
-    sel_recv,
     xg_send,
     xg_recv,
     xr_send,
     xr_recv,
-    y_send,
-    y_recv,
 ):
     nz, nx, cap, rows, cols, pad = cfg
     half = nz // 2
@@ -69,7 +60,6 @@
     ep = lax.axis_index("ep")
     x = lax.axis_index("tp")
     z, c = ep // CORES, ep % CORES
-    f = 1 - 2 * c
 
     def wrap(v, n):
         return lax.rem(v + 2 * n, n)
@@ -78,10 +68,11 @@
         {"ep": wrap(z + 1, nz) * CORES + c},
         {"ep": wrap(z - 1, nz) * CORES + c},
     )
-    sib = {"ep": z * CORES + 1 - c}
-    x_up, x_dn = {"tp": wrap(x + 1, nx)}, {"tp": wrap(x - 1, nx)}
-    x_f, x_b = wrap(x + f, nx), wrap(x - f, nx)
-    x_far = wrap(x + 2, nx)
+    sib = z * CORES + 1 - c
+    near, far_side = pl.ds(0, 2 * cap), pl.ds(2 * cap, 2 * cap)
+
+    peers = [{"tp": wrap(x + r, nx)} for r in range(1, nx)]
+    peers += [{"tp": wrap(x + r, nx), "ep": sib} for r in range(nx)]
 
     def reach(d):
         return half - jnp.where(c == d, 0, 1)
@@ -114,38 +105,49 @@
             rs_send.at[d, par, j], rs_recv.at[d, h - 1, j], z_to[1 - d],
         )
 
-    def sel_copy(h):
+    def live(base, core, last):
+        if last:
+            return pl.ds(pl.multiple_of(base + core * cap, cap), cap)
+        return pl.ds(base, 2 * cap)
+
+    def xg_copy(h, n, last):
+        own = n < nx - 1
+        src = grow.at[x, h, live(0, c, last)] if own else stg.at[h, live(0, c, last)]
+        dst = grow.at[x, h, live(0 if own else 2 * cap, c, last)]
+        return remote(src, dst, xg_send.at[h, n], xg_recv.at[h, n], peers[n])
+
+    def xr_copy(h, n, last):
+        own = n < nx - 1
+        to = wrap(x + n + 1, nx) if own else wrap(x + n + 1 - nx, nx)
+        core = c if own else 1 - c
+        src = part.at[h, to, live(0 if own else 2 * cap, core, last)]
+        dst = in_own.at[h, n] if own else in_sib.at[h, n + 1 - nx]
         return remote(
-            stg.at[h], grow.at[x, h, pl.ds(2 * cap, 2 * cap)], sel_send.at[h], sel_recv.at[h], sib
+            src, dst.at[live(0, core, last)], xr_send.at[h, n], xr_recv.at[h, n], peers[n]
         )
 
-    def xg_copy(h, way):
-        if way == 0:
-            return remote(grow.at[x, h], grow.at[x, h], xg_send.at[h, 0], xg_recv.at[h, 0], x_up)
-        if way == 1:
-            return remote(grow.at[x, h], grow.at[x, h], xg_send.at[h, 1], xg_recv.at[h, 1], x_dn)
-        return remote(
-            grow.at[x_b, h], grow.at[x_b, h], xg_send.at[h, 2], xg_recv.at[h, 2], {"tp": x_f}
-        )
-
-    def xr_copy(h, way):
-        if way == 0:
-            return remote(
-                part.at[h, x_far], relay.at[h], xr_send.at[h, 0], xr_recv.at[h, 0], {"tp": x_f}
-            )
-        if way == 1:
-            return remote(
-                part.at[h, x_b], direct.at[h], xr_send.at[h, 1], xr_recv.at[h, 1], {"tp": x_b}
-            )
-        return remote(
-            pair.at[h], pair_in.at[h], xr_send.at[h, 2], xr_recv.at[h, 2], {"tp": x_f}
-        )
-
-    def y_copy(h):
-        return remote(y_out.at[h], y_sib.at[h], y_send.at[h], y_recv.at[h], sib)
+    def for_peers(copy, h, act):
+        @pl.when(h == half)
+        def _():
+            for n in range(len(peers)):
+                act(copy(h, n, True))
+
+        @pl.when(h != half)
+        def _():
+            for n in range(len(peers)):
+                act(copy(h, n, False))
+
+    def start(copy):
+        copy.start()
+
+    def arrived(copy):
+        copy.wait_recv()
+
+    def left(copy):
+        copy.wait_send()
 
     barrier = pltpu.get_barrier_semaphore()
-    for dev in (*z_to, sib, x_up, x_dn):
+    for dev in (*z_to, *peers):
         pl.semaphore_signal(barrier, inc=1, device_id=dev, device_id_type=MESH)
 
     load = pltpu.make_async_copy(tok_hbm, tok, w_sem.at[3])
@@ -157,6 +159,13 @@
     for copy in weights:
         copy.start()
 
+    idle = jnp.zeros((cap, cols), BF16)
+    for r in range(nx):
+        grow[r, half, live(0, 1 - c, True)] = idle
+        grow[r, half, live(2 * cap, c, True)] = idle
+        in_sib[half, r, live(0, 1 - c, True)] = idle
+        if r < nx - 1:
+            in_own[half, r, live(0, 1 - c, True)] = idle
     for d in range(2):
         for j in range(PARTS + 1):
             low = half - 1 - (0 if j == PARTS else (sub * j) // (CORES * cap))
@@ -171,14 +180,7 @@
                         if j < PARTS:
                             ag[d, h, pl.ds(j * sub, sub)] = jnp.zeros((sub, cols), BF16)
                         else:
-                            agm[d, h] = jnp.full((8, pad), -1.0, F32)
-
-    load.wait()
-    widened = tok[...].astype(F32)
-    scale = lax.rsqrt(jnp.mean(widened * widened, axis=-1, keepdims=True) + epsilon)
-    mine = pl.ds(pl.multiple_of(x * cols, cols), cols)
-    own_cols = tok[:, mine].astype(F32) * scale
-    own_cols = (own_cols * gain_ref[:, mine]).astype(BF16)
+                            agm[d, h] = jnp.full((8, pad), -1.0, BF16)
 
     meta = meta_ref[...]
     ids = meta[0:4].astype(jnp.int32)
@@ -187,6 +189,7 @@
     behind = jnp.where(ahead == 0, 0, nz - ahead)
     lane = lax.broadcasted_iota(jnp.int32, (pad, pad), 1)
     line = lax.broadcasted_iota(jnp.int32, (pad, pad), 0)
+    orders = []
     for d, dist in enumerate((ahead, behind)):
         far = jnp.max(jnp.where(dist <= reach(d), dist, 0), axis=0, keepdims=True)
         far = jnp.where(lane[0:1] < rows, far, -1).astype(F32)
@@ -198,13 +201,22 @@
         rank_line = jnp.sum(jnp.where(later, 1.0, 0.0), axis=1, keepdims=True)
         order = jnp.where(rank_lane == line.astype(F32), 1.0, 0.0).astype(BF16)
         back_to = jnp.where(rank_line == lane.astype(F32), 1.0, 0.0).astype(BF16)
-        ag[d, 0] = jnp.dot(
-            order[:rows, :rows], own_cols, preferred_element_type=F32
+        orders.append(order[:rows, :rows])
+        agm[d, 0] = jnp.dot(
+            meta.astype(BF16), back_to, preferred_element_type=F32
         ).astype(BF16)
-        agm[d, 0] = jnp.dot(meta.astype(BF16), back_to, preferred_element_type=F32)
         back[d] = back_to
 
-    pl.semaphore_wait(barrier, 5)
+    load.wait()
+    widened = tok[...].astype(F32)
+    scale = lax.rsqrt(jnp.mean(widened * widened, axis=-1, keepdims=True) + epsilon)
+    mine = pl.ds(pl.multiple_of(x * cols, cols), cols)
+    own_cols = tok[:, mine].astype(F32) * scale
+    own_cols = (own_cols * gain_ref[:, mine]).astype(BF16)
+    for d in range(2):
+        ag[d, 0] = jnp.dot(orders[d], own_cols, preferred_element_type=F32).astype(BF16)
+
+    pl.semaphore_wait(barrier, 2 + len(peers))
 
     sub_line = lax.broadcasted_iota(jnp.int32, (2 * cap, pad), 0)
     own_slot = jnp.where(sub_line < cap, sub_line, sub_line - cap).astype(F32)
@@ -213,9 +225,9 @@
         valid = h <= reach(d)
         if d == 1:
             valid = valid & (h >= 1)
-        expert = jnp.where(sub_line < cap, ep, z * CORES + 1 - c)
+        expert = jnp.where(sub_line < cap, ep, sib)
         expert = jnp.where(valid, expert, -7).astype(F32)
-        meta = agm[d, h]
+        meta = agm[d, h].astype(F32)
         named = jnp.zeros((2 * cap, pad), F32)
         weight = jnp.zeros((2 * cap, pad), F32)
         for k in range(4):
@@ -245,54 +257,43 @@
         stg[h, pl.ds(d * cap, cap)] = got[cap:]
 
     def dispatch(i, _):
-        @pl.when(i <= half)
-        def _():
-            for j in (PARTS, *range(PARTS)):
-                for d in range(2):
-                    @pl.when((i >= 1) & (i <= hops(d, j)))
-                    def _():
-                        ag_copy(d, i - 1, j).wait_recv()
-
-                    @pl.when(i < hops(d, j))
-                    def _():
-                        @pl.when(i >= 2)
-                        def _():
-                            ag_copy(d, i - 2, j).wait_send()
-
-                        ag_copy(d, i, j).start()
-
-        @pl.when((i >= 1) & (i <= half + 1))
-        def _():
-            h = i - 1
-            sel_copy(h).wait_recv()
-            xg_copy(h, 0).start()
-            xg_copy(h, 1).start()
-
-        @pl.when(i <= half)
-        def _():
-            select(0, i)
-            select(1, i)
-            sel_copy(i).start()
-
-        @pl.when(i >= 2)
-        def _():
-            h = i - 2
-            remote(
-                grow.at[x_b, h], grow.at[x_b, h], xg_send.at[h, 2], xg_recv.at[h, c], x_up
-            ).wait_recv()
-            xg_copy(h, 2).start()
-
+        for j in (PARTS, *range(PARTS)):
+            for d in range(2):
+                @pl.when((i >= 1) & (i <= hops(d, j)))
+                def _():
+                    ag_copy(d, i - 1, j).wait_recv()
+
+                @pl.when(i < hops(d, j))
+                def _():
+                    @pl.when(i >= 2)
+                    def _():
+                        ag_copy(d, i - 2, j).wait_send()
+
+                    ag_copy(d, i, j).start()
+
+        select(0, i)
+        select(1, i)
+        for_peers(xg_copy, i, start)
         return 0
 
-    lax.fori_loop(0, half + 3, dispatch, 0)
+    lax.fori_loop(0, half + 1, dispatch, 0)
 
     for copy in weights:
         copy.wait()
 
     def spread_out(h):
+        for_peers(xr_copy, h, arrived)
+        y_own = part[h, x, near].astype(F32)
+        y_sib = jnp.zeros_like(y_own)
+        for r in range(nx):
+            if r < nx - 1:
+                y_own = y_own + in_own[h, r].astype(F32)
+            y_sib = y_sib + in_sib[h, r].astype(F32)
+        y_own, y_sib = y_own.astype(BF16), y_sib.astype(BF16)
         for d in range(2):
-            mid = pl.ds(d * cap, cap)
-            both = jnp.concatenate([y_own[h, mid], y_sib[h, mid]], axis=0)
+            both = jnp.concatenate(
+                [y_own[d * cap : (d + 1) * cap], y_sib[d * cap : (d + 1) * cap]], axis=0
+            )
             gains[d] = jnp.dot(cbuf[d, h], both, preferred_element_type=F32)
 
     def blend(d, h, j):
@@ -300,10 +301,9 @@
         return rs[d, h, win].astype(F32) + gains[d, win]
 
     def gather_back(i, _):
-        @pl.when(i >= 3)
+        @pl.when(i >= 2)
         def _():
-            h = half - i + 3
-            y_copy(h).wait_recv()
+            h = half - i + 2
             spread_out(h)
             for j in range(PARTS):
                 for d in range(2):
@@ -323,10 +323,7 @@
         @pl.when(i <= half)
         def _():
             h = half - i
-            remote(
-                grow.at[x_f, h], grow.at[x_f, h], xg_send.at[h, 2], xg_recv.at[h, 1 - c], x_up
-            ).wait_recv()
-            xg_copy(h, 2).wait_recv()
+            for_peers(xg_copy, h, arrived)
             gate = jnp.zeros((4 * cap, wg.shape[1]), F32)
             up = jnp.zeros((4 * cap, wg.shape[1]), F32)
             for k in range(nx):
@@ -342,33 +339,12 @@
                 part[h, k] = jnp.dot(
                     active, wd[:, pl.ds(k * cols, cols)], preferred_element_type=F32
                 ).astype(BF16)
-            xr_copy(h, 0).start()
-            xr_copy(h, 1).start()
-
-        @pl.when((i >= 1) & (i <= half + 1))
-        def _():
-            h = half - i + 1
-            xr_copy(h, 0).wait_recv()
-            pair[h] = (part[h, x_f].astype(F32) + relay[h].astype(F32)).astype(BF16)
-            xr_copy(h, 2).start()
-
-        @pl.when((i >= 2) & (i <= half + 2))
-        def _():
-            h = half - i + 2
-            xr_copy(h, 1).wait_recv()
-            xr_copy(h, 2).wait_recv()
-            total = (
-                part[h, x].astype(F32) + direct[h].astype(F32) + pair_in[h].astype(F32)
-            ).astype(BF16)
-            y_own[h] = total[: 2 * cap]
-            y_out[h] = total[2 * cap :]
-            y_copy(h).start()
+            for_peers(xr_copy, h, start)
 
         return 0
 
-    lax.fori_loop(0, half + 3, gather_back, 0)
-
-    y_copy(0).wait_recv()
+    lax.fori_loop(0, half + 2, gather_back, 0)
+
     spread_out(0)
     total = jnp.zeros((rows, cols), F32)
     for d in range(2):
@@ -394,11 +370,8 @@
                         rs_copy(d, k, j).wait_send()
 
     def drain(h, _):
-        sel_copy(h).wait_send()
-        y_copy(h).wait_send()
-        for way in range(3):
-            xg_copy(h, way).wait_send()
-            xr_copy(h, way).wait_send()
+        for_peers(xg_copy, h, left)
+        for_peers(xr_copy, h, left)
         return 0
 
     lax.fori_loop(0, half + 1, drain, 0)
@@ -426,19 +399,14 @@
         out_specs=vmem,
         scratch_shapes=[
             pltpu.VMEM((2, steps, rows, cols), BF16),
-            pltpu.VMEM((2, steps, 8, pad), F32),
+            pltpu.VMEM((2, steps, 8, pad), BF16),
             pltpu.VMEM((2, steps, rows, cols), BF16),
             pltpu.VMEM((2, 2, rows, cols), BF16),
             pltpu.VMEM((tp_count, steps, *block), BF16),
             pltpu.VMEM((steps, 2 * cap, cols), BF16),
             pltpu.VMEM((steps, tp_count, *block), BF16),
-            pltpu.VMEM((steps, *block), BF16),
-            pltpu.VMEM((steps, *block), BF16),
-            pltpu.VMEM((steps, *block), BF16),
-            pltpu.VMEM((steps, *block), BF16),
-            pltpu.VMEM((steps, 2 * cap, cols), BF16),
-            pltpu.VMEM((steps, 2 * cap, cols), BF16),
-            pltpu.VMEM((steps, 2 * cap, cols), BF16),
+            pltpu.VMEM((steps, tp_count - 1, 2 * cap, cols), BF16),
+            pltpu.VMEM((steps, tp_count, 2 * cap, cols), BF16),
             pltpu.VMEM((2, steps, rows, 2 * cap), BF16),
             pltpu.VMEM((2, rows, cols), F32),
             pltpu.VMEM((2, pad, pad), BF16),
@@ -451,14 +419,10 @@
             dma((2, steps, PARTS + 1)),
             dma((2, 2, PARTS)),
             dma((2, steps, PARTS)),
-            dma((steps,)),
-            dma((steps,)),
-            dma((steps, 3)),
-            dma((steps, 3)),
-            dma((steps, 3)),
-            dma((steps, 3)),
-            dma((steps,)),
-            dma((steps,)),
+            dma((steps, 2 * tp_count - 1)),
+            dma((steps, 2 * tp_count - 1)),
+            dma((steps, 2 * tp_count - 1)),
+            dma((steps, 2 * tp_count - 1)),
         ],
         compiler_params=pltpu.CompilerParams(
             collective_id=0, has_side_effects=True, vmem_limit_bytes=60 * 1024 * 1024

time: 210 us -> 202 us (0.962)
  Pallas kernels: 207 us -> 199 us
    pallas_call x1, Pallas kernels: 207 us -> 199 us  [body(): pl.pallas_call(functools.partial(kernel, (ep_count // CORES, tp_count, ca...]
where the time goes in v3:
time: 202 us; the launch traced here: 201 us
  Pallas kernels  199 us (99%)
    pallas_call x1, Pallas kernels, body(): pl.pallas_call(functools.partial(kernel, (ep_count // CORES, tp_count, ca...  199 us

profile of v3, /device:TPU:33, one launch (start us, length us, event | category | flops | bytes accessed | tf_op | source)
XLA Modules:
  0.0 201.5 jit_solution(5890733728482142209)
XLA Ops:
  0.0 0.0 copy-start
  0.0 0.7 convert_bitcast_fusion
  0.7 0.0 copy-done
  0.7 0.6 select_maximum_fusion.meta_ref
  1.3 198.5 %shard_map.73 = bf16[192,512]{1,0:T(8,128)(2,1)} custom-call(bf16[192,2048]{1,0:T(8,128)(2,1)} %tok_hbm.1, f32[1,2048]{1,0:T(1,128)} %bitcast.4, f32[8,256]{1,0:T(8,128)} %select_maximum_fusion.meta_ref, bf16[1,2048,256]{2,1,0:T(8,128)(2,1)} %wg_hbm.1, bf16[1,2048,256]{2,1,0:T(8,128)(2,1)} %wu_hbm.1, bf16[1,256,2048]{2,1,0:T(8,128)(2,1)} %wd_hbm.1), custom_call_target="tpu_custom_call" | custom-call | tf_op jit(solution)/shard_map/pallas_call | solution.py:395
  199.9 1.6 copy.9
Async XLA Ops:
  0.0 0.7 copy-start

commit v4 on v3

--- a/solution.py
+++ b/solution.py
@@ -22,8 +22,9 @@
 def kernel(
     cfg,
     tok_hbm,
-    gain_ref,
-    meta_ref,
+    gain_hbm,
+    ids_hbm,
+    gate_hbm,
     wg_hbm,
     wu_hbm,
     wd_hbm,
@@ -35,12 +36,15 @@
     grow,
     stg,
     part,
-    in_own,
-    in_sib,
+    inbox,
     cbuf,
     gains,
     back,
     tok,
+    gain,
+    ids_in,
+    gate_in,
+    meta_in,
     wg,
     wu,
     wd,
@@ -71,8 +75,11 @@
     sib = z * CORES + 1 - c
     near, far_side = pl.ds(0, 2 * cap), pl.ds(2 * cap, 2 * cap)
 
-    peers = [{"tp": wrap(x + r, nx)} for r in range(1, nx)]
-    peers += [{"tp": wrap(x + r, nx), "ep": sib} for r in range(nx)]
+    moves = [(r, own) for r in range(nx) for own in (True, False) if r or not own]
+    moves.sort(key=lambda m: -min(m[0], nx - m[0]))
+    peers = [
+        {"tp": wrap(x + r, nx)} if own else {"tp": wrap(x + r, nx), "ep": sib} for r, own in moves
+    ]
 
     def reach(d):
         return half - jnp.where(c == d, 0, 1)
@@ -111,20 +118,17 @@
         return pl.ds(base, 2 * cap)
 
     def xg_copy(h, n, last):
-        own = n < nx - 1
+        own = moves[n][1]
         src = grow.at[x, h, live(0, c, last)] if own else stg.at[h, live(0, c, last)]
         dst = grow.at[x, h, live(0 if own else 2 * cap, c, last)]
         return remote(src, dst, xg_send.at[h, n], xg_recv.at[h, n], peers[n])
 
     def xr_copy(h, n, last):
-        own = n < nx - 1
-        to = wrap(x + n + 1, nx) if own else wrap(x + n + 1 - nx, nx)
+        r, own = moves[n]
         core = c if own else 1 - c
-        src = part.at[h, to, live(0 if own else 2 * cap, core, last)]
-        dst = in_own.at[h, n] if own else in_sib.at[h, n + 1 - nx]
-        return remote(
-            src, dst.at[live(0, core, last)], xr_send.at[h, n], xr_recv.at[h, n], peers[n]
-        )
+        src = part.at[h, wrap(x + r, nx), live(0 if own else 2 * cap, core, last)]
+        dst = inbox.at[h, n, live(0, core, last)]
+        return remote(src, dst, xr_send.at[h, n], xr_recv.at[h, n], peers[n])
 
     def for_peers(copy, h, act):
         @pl.when(h == half)
@@ -150,8 +154,14 @@
     for dev in (*z_to, *peers):
         pl.semaphore_signal(barrier, inc=1, device_id=dev, device_id_type=MESH)
 
-    load = pltpu.make_async_copy(tok_hbm, tok, w_sem.at[3])
-    load.start()
+    loads = [
+        pltpu.make_async_copy(src, dst, w_sem.at[3 + k])
+        for k, (src, dst) in enumerate(
+            ((ids_hbm, ids_in), (gate_hbm, gate_in), (tok_hbm, tok), (gain_hbm, gain))
+        )
+    ]
+    for copy in loads:
+        copy.start()
     weights = [
         pltpu.make_async_copy(src.at[0], dst, w_sem.at[k])
         for k, (src, dst) in enumerate(((wg_hbm, wg), (wu_hbm, wu), (wd_hbm, wd)))
@@ -163,9 +173,8 @@
     for r in range(nx):
         grow[r, half, live(0, 1 - c, True)] = idle
         grow[r, half, live(2 * cap, c, True)] = idle
-        in_sib[half, r, live(0, 1 - c, True)] = idle
-        if r < nx - 1:
-            in_own[half, r, live(0, 1 - c, True)] = idle
+    for n in range(len(peers)):
+        inbox[half, n, live(0, 1 - c, True)] = idle
     for d in range(2):
         for j in range(PARTS + 1):
             low = half - 1 - (0 if j == PARTS else (sub * j) // (CORES * cap))
@@ -182,7 +191,12 @@
                         else:
                             agm[d, h] = jnp.full((8, pad), -1.0, BF16)
 
-    meta = meta_ref[...]
+    meta_in[...] = jnp.full((8, pad), -1.0, F32)
+    loads[0].wait()
+    loads[1].wait()
+    meta_in[0:4, 0:rows] = ids_in[...].astype(F32)
+    meta_in[4:8, 0:rows] = gate_in[...]
+    meta = meta_in[...]
     ids = meta[0:4].astype(jnp.int32)
     ahead = lax.shift_right_arithmetic(ids, 1) - z
     ahead = jnp.where(ahead < 0, ahead + nz, ahead)
@@ -207,14 +221,18 @@
         ).astype(BF16)
         back[d] = back_to
 
-    load.wait()
+    loads[2].wait()
+    loads[3].wait()
     widened = tok[...].astype(F32)
     scale = lax.rsqrt(jnp.mean(widened * widened, axis=-1, keepdims=True) + epsilon)
     mine = pl.ds(pl.multiple_of(x * cols, cols), cols)
     own_cols = tok[:, mine].astype(F32) * scale
-    own_cols = (own_cols * gain_ref[:, mine]).astype(BF16)
+    own_cols = (own_cols * gain[:, mine]).astype(BF16)
     for d in range(2):
         ag[d, 0] = jnp.dot(orders[d], own_cols, preferred_element_type=F32).astype(BF16)
+
+    for copy in weights:
+        copy.wait()
 
     pl.semaphore_wait(barrier, 2 + len(peers))
 
@@ -256,6 +274,24 @@
         grow[x, h, pl.ds(d * cap, cap)] = got[:cap]
         stg[h, pl.ds(d * cap, cap)] = got[cap:]
 
+    def expert(h):
+        for_peers(xg_copy, h, arrived)
+        gate = jnp.zeros((4 * cap, wg.shape[1]), F32)
+        up = jnp.zeros((4 * cap, wg.shape[1]), F32)
+        for k in range(nx):
+            block = grow[k, h]
+            gate = gate + jnp.dot(
+                block, wg[pl.ds(k * cols, cols)], preferred_element_type=F32
+            )
+            up = up + jnp.dot(block, wu[pl.ds(k * cols, cols)], preferred_element_type=F32)
+        gated = jnp.minimum(gate, clamp_limit)
+        linear = jnp.clip(up, -clamp_limit, clamp_limit)
+        active = (gated * jax.nn.sigmoid(swish_alpha * gated) * (linear + 1.0)).astype(BF16)
+        for k in range(nx):
+            part[h, k] = jnp.dot(
+                active, wd[:, pl.ds(k * cols, cols)], preferred_element_type=F32
+            ).astype(BF16)
+
     def dispatch(i, _):
         for j in (PARTS, *range(PARTS)):
             for d in range(2):
@@ -271,24 +307,29 @@
 
                     ag_copy(d, i, j).start()
 
-        select(0, i)
-        select(1, i)
+        for d in range(2):
+            @pl.when(i <= reach(d))
+            def _():
+                select(d, i)
+
         for_peers(xg_copy, i, start)
+        @pl.when(i >= 2)
+        def _():
+            expert(i - 2)
+
         return 0
 
     lax.fori_loop(0, half + 1, dispatch, 0)
-
-    for copy in weights:
-        copy.wait()
 
     def spread_out(h):
         for_peers(xr_copy, h, arrived)
         y_own = part[h, x, near].astype(F32)
         y_sib = jnp.zeros_like(y_own)
-        for r in range(nx):
-            if r < nx - 1:
-                y_own = y_own + in_own[h, r].astype(F32)
-            y_sib = y_sib + in_sib[h, r].astype(F32)
+        for n, (_, own) in enumerate(moves):
+            if own:
+                y_own = y_own + inbox[h, n].astype(F32)
+            else:
+                y_sib = y_sib + inbox[h, n].astype(F32)
         y_own, y_sib = y_own.astype(BF16), y_sib.astype(BF16)
         for d in range(2):
             both = jnp.concatenate(
@@ -304,6 +345,11 @@
         @pl.when(i >= 2)
         def _():
             h = half - i + 2
+
+            @pl.when(h + 2 <= half)
+            def _():
+                for_peers(xr_copy, h + 2, left)
+
             spread_out(h)
             for j in range(PARTS):
                 for d in range(2):
@@ -323,27 +369,25 @@
         @pl.when(i <= half)
         def _():
             h = half - i
-            for_peers(xg_copy, h, arrived)
-            gate = jnp.zeros((4 * cap, wg.shape[1]), F32)
-            up = jnp.zeros((4 * cap, wg.shape[1]), F32)
-            for k in range(nx):
-                block = grow[k, h]
-                gate = gate + jnp.dot(
-                    block, wg[pl.ds(k * cols, cols)], preferred_element_type=F32
-                )
-                up = up + jnp.dot(block, wu[pl.ds(k * cols, cols)], preferred_element_type=F32)
-            gated = jnp.minimum(gate, clamp_limit)
-            linear = jnp.clip(up, -clamp_limit, clamp_limit)
-            active = (gated * jax.nn.sigmoid(swish_alpha * gated) * (linear + 1.0)).astype(BF16)
-            for k in range(nx):
-                part[h, k] = jnp.dot(
-                    active, wd[:, pl.ds(k * cols, cols)], preferred_element_type=F32
-                ).astype(BF16)
+            @pl.when(i < 2)
+            def _():
+                expert(h)
+
             for_peers(xr_copy, h, start)
+            for_peers(xg_copy, h, left)
 
         return 0
 
     lax.fori_loop(0, half + 2, gather_back, 0)
+
+    for h in range(min(3, half + 1)):
+        for_peers(xr_copy, h, left)
+    for d in range(2):
+        for j in range(PARTS + 1):
+            for k in (1, 2):
+                @pl.when(hops(d, j) >= k)
+                def _():
+                    ag_copy(d, hops(d, j) - k, j).wait_send()
 
     spread_out(0)
     total = jnp.zeros((rows, cols), F32)
@@ -359,22 +403,11 @@
     out_ref[...] = total.astype(BF16)
 
     for d in range(2):
-        for j in range(PARTS + 1):
+        for j in range(PARTS):
             for k in (1, 2):
                 @pl.when(hops(d, j) >= k)
                 def _():
-                    ag_copy(d, hops(d, j) - k, j).wait_send()
-                if j < PARTS:
-                    @pl.when(hops(d, j) >= k)
-                    def _():
-                        rs_copy(d, k, j).wait_send()
-
-    def drain(h, _):
-        for_peers(xg_copy, h, left)
-        for_peers(xr_copy, h, left)
-        return 0
-
-    lax.fori_loop(0, half + 1, drain, 0)
+                    rs_copy(d, k, j).wait_send()
 
 
 def body(ep_count, tp_count, tokens, norm_gain, w_gate, w_up, w_down, expert_ids, gate_weights):
@@ -386,8 +419,6 @@
     hidden = w_gate.shape[2]
     pad = -(-rows // 128) * 128
     steps = ep_count // CORES // 2 + 1
-    meta = jnp.concatenate([expert_ids.astype(F32).T, gate_weights.T], axis=0)
-    meta = jnp.pad(meta, ((0, 0), (0, pad - rows)), constant_values=-1.0)
     vmem = pl.BlockSpec(memory_space=pltpu.VMEM)
     hbm = pl.BlockSpec(memory_space=pl.ANY)
     dma = pltpu.SemaphoreType.DMA
@@ -395,7 +426,7 @@
     return pl.pallas_call(
         functools.partial(kernel, (ep_count // CORES, tp_count, cap, rows, cols, pad)),
         out_shape=jax.ShapeDtypeStruct((rows, cols), BF16),
-        in_specs=[hbm, vmem, vmem, hbm, hbm, hbm],
+        in_specs=[hbm] * 7,
         out_specs=vmem,
         scratch_shapes=[
             pltpu.VMEM((2, steps, rows, cols), BF16),
@@ -405,16 +436,19 @@
             pltpu.VMEM((tp_count, steps, *block), BF16),
             pltpu.VMEM((steps, 2 * cap, cols), BF16),
             pltpu.VMEM((steps, tp_count, *block), BF16),
-            pltpu.VMEM((steps, tp_count - 1, 2 * cap, cols), BF16),
-            pltpu.VMEM((steps, tp_count, 2 * cap, cols), BF16),
+            pltpu.VMEM((steps, 2 * tp_count - 1, 2 * cap, cols), BF16),
             pltpu.VMEM((2, steps, rows, 2 * cap), BF16),
             pltpu.VMEM((2, rows, cols), F32),
             pltpu.VMEM((2, pad, pad), BF16),
             pltpu.VMEM((rows, width), BF16),
+            pltpu.VMEM((1, width), F32),
+            pltpu.VMEM((top, rows), jnp.int32),
+            pltpu.VMEM((top, rows), F32),
+            pltpu.VMEM((8, pad), F32),
             pltpu.VMEM((width, hidden), BF16),
             pltpu.VMEM((width, hidden), BF16),
             pltpu.VMEM((hidden, width), BF16),
-            dma((4,)),
+            dma((7,)),
             dma((2, 2, PARTS + 1)),
             dma((2, steps, PARTS + 1)),
             dma((2, 2, PARTS)),
@@ -427,7 +461,7 @@
         compiler_params=pltpu.CompilerParams(
             collective_id=0, has_side_effects=True, vmem_limit_bytes=60 * 1024 * 1024
         ),
-    )(tokens, norm_gain.reshape(1, width), meta, w_gate, w_up, w_down)
+    )(tokens, norm_gain.reshape(1, width), expert_ids.T, gate_weights.T, w_gate, w_up, w_down)
 
 
 def solution(mesh):

time: 202 us -> 198 us (0.980)
  Pallas kernels: 199 us -> 196 us
    pallas_call x1, Pallas kernels: 199 us -> 196 us  [body(): pl.pallas_call(functools.partial(kernel, (ep_count // CORES, tp_count, ca...]
where the time goes in v4:
time: 198 us
  Pallas kernels  196 us (99%)
    pallas_call x1, Pallas kernels, body(): pl.pallas_call(functools.partial(kernel, (ep_count // CORES, tp_count, ca...  196 us

profile of v4, /device:TPU:33, one launch (start us, length us, event | category | flops | bytes accessed | tf_op | source)
XLA Modules:
  0.0 198.0 jit_solution(7482511827905789611)
XLA Ops:
  0.0 196.4 %shard_map.73 = bf16[192,512]{1,0:T(8,128)(2,1)} custom-call(bf16[192,2048]{1,0:T(8,128)(2,1)} %tok_hbm.1, f32[1,2048]{1,0:T(1,128)} %bitcast.3, s32[4,192]{1,0:T(4,128)} %bitcast.4, f32[4,192]{1,0:T(4,128)} %bitcast.5, bf16[1,2048,256]{2,1,0:T(8,128)(2,1)} %wg_hbm.1, bf16[1,2048,256]{2,1,0:T(8,128)(2,1)} %wu_hbm.1, bf16[1,256,2048]{2,1,0:T(8,128)(2,1)} %wd_hbm.1), custom_call_target="tpu_custom_call" | custom-call | tf_op jit(solution)/shard_map/pallas_call | solution.py:426
  196.4 1.6 copy.9

commit v5 on v4

--- a/solution.py
+++ b/solution.py
@@ -16,6 +16,7 @@
 swish_alpha = 1.702
 
 CORES = 2
+AHEAD = 4
 PARTS = 6
 
 
@@ -321,6 +322,12 @@
 
     lax.fori_loop(0, half + 1, dispatch, 0)
 
+    def last_experts(k, _):
+        expert(half - 1 + k)
+        return 0
+
+    lax.fori_loop(0, 2, last_experts, 0)
+
     def spread_out(h):
         for_peers(xr_copy, h, arrived)
         y_own = part[h, x, near].astype(F32)
@@ -342,9 +349,15 @@
         return rs[d, h, win].astype(F32) + gains[d, win]
 
     def gather_back(i, _):
-        @pl.when(i >= 2)
+        @pl.when(i <= half)
         def _():
-            h = half - i + 2
+            h = half - i
+            for_peers(xr_copy, h, start)
+            for_peers(xg_copy, h, left)
+
+        @pl.when(i >= AHEAD)
+        def _():
+            h = half - i + AHEAD
 
             @pl.when(h + 2 <= half)
             def _():
@@ -366,19 +379,9 @@
                         rsend[d, lax.rem(h, 2), pl.ds(j * sub, sub)] = blend(d, h, j).astype(BF16)
                         rs_copy(d, h, j).start()
 
-        @pl.when(i <= half)
-        def _():
-            h = half - i
-            @pl.when(i < 2)
-            def _():
-                expert(h)
-
-            for_peers(xr_copy, h, start)
-            for_peers(xg_copy, h, left)
-
         return 0
 
-    lax.fori_loop(0, half + 2, gather_back, 0)
+    lax.fori_loop(0, half + AHEAD, gather_back, 0)
 
     for h in range(min(3, half + 1)):
         for_peers(xr_copy, h, left)

time: 198 us -> 198 us (level)
  no operation moved by 1% of the time
where the time goes in v5:
time: 198 us; the launch traced here: 197 us
  Pallas kernels  195 us (98%)
    pallas_call x1, Pallas kernels, body(): pl.pallas_call(functools.partial(kernel, (ep_count // CORES, tp_count, ca...  195 us

profile of v5, /device:TPU:33, one launch (start us, length us, event | category | flops | bytes accessed | tf_op | source)
XLA Modules:
  0.0 196.7 jit_solution(13857440695326324171)
XLA Ops:
  0.0 195.1 %shard_map.73 = bf16[192,512]{1,0:T(8,128)(2,1)} custom-call(bf16[192,2048]{1,0:T(8,128)(2,1)} %tok_hbm.1, f32[1,2048]{1,0:T(1,128)} %bitcast.3, s32[4,192]{1,0:T(4,128)} %bitcast.4, f32[4,192]{1,0:T(4,128)} %bitcast.5, bf16[1,2048,256]{2,1,0:T(8,128)(2,1)} %wg_hbm.1, bf16[1,2048,256]{2,1,0:T(8,128)(2,1)} %wu_hbm.1, bf16[1,256,2048]{2,1,0:T(8,128)(2,1)} %wd_hbm.1), custom_call_target="tpu_custom_call" | custom-call | tf_op jit(solution)/shard_map/pallas_call | solution.py:429
  195.1 1.6 copy.9

commit v6 on v5

--- a/solution.py
+++ b/solution.py
@@ -314,19 +314,19 @@
                 select(d, i)
 
         for_peers(xg_copy, i, start)
-        @pl.when(i >= 2)
+        @pl.when(i >= 3)
         def _():
-            expert(i - 2)
+            expert(i - 3)
 
         return 0
 
     lax.fori_loop(0, half + 1, dispatch, 0)
 
     def last_experts(k, _):
-        expert(half - 1 + k)
+        expert(half - 2 + k)
         return 0
 
-    lax.fori_loop(0, 2, last_experts, 0)
+    lax.fori_loop(0, 3, last_experts, 0)
 
     def spread_out(h):
         for_peers(xr_copy, h, arrived)

time: 198 us -> 197 us (level)
  no operation moved by 1% of the time
where the time goes in v6:
time: 197 us; the launch traced here: 196 us
  Pallas kernels  194 us (98%)
    pallas_call x1, Pallas kernels, body(): pl.pallas_call(functools.partial(kernel, (ep_count // CORES, tp_count, ca...  194 us

profile of v6, /device:TPU:33, one launch (start us, length us, event | category | flops | bytes accessed | tf_op | source)
XLA Modules:
  0.0 195.7 jit_solution(9816215343510866671)
XLA Ops:
  0.0 194.1 %shard_map.73 = bf16[192,512]{1,0:T(8,128)(2,1)} custom-call(bf16[192,2048]{1,0:T(8,128)(2,1)} %tok_hbm.1, f32[1,2048]{1,0:T(1,128)} %bitcast.3, s32[4,192]{1,0:T(4,128)} %bitcast.4, f32[4,192]{1,0:T(4,128)} %bitcast.5, bf16[1,2048,256]{2,1,0:T(8,128)(2,1)} %wg_hbm.1, bf16[1,2048,256]{2,1,0:T(8,128)(2,1)} %wu_hbm.1, bf16[1,256,2048]{2,1,0:T(8,128)(2,1)} %wd_hbm.1), custom_call_target="tpu_custom_call" | custom-call | tf_op jit(solution)/shard_map/pallas_call | solution.py:429
  194.1 1.6 copy.9

commit v7 on v6

--- a/solution.py
+++ b/solution.py
@@ -16,7 +16,7 @@
 swish_alpha = 1.702
 
 CORES = 2
-AHEAD = 4
+AHEAD = 5
 PARTS = 6
 
 

time: 197 us -> 197 us (level)
  no operation moved by 1% of the time
where the time goes in v7:
time: 197 us; the launch traced here: 196 us
  Pallas kernels  194 us (98%)
    pallas_call x1, Pallas kernels, body(): pl.pallas_call(functools.partial(kernel, (ep_count // CORES, tp_count, ca...  194 us

profile of v7, /device:TPU:33, one launch (start us, length us, event | category | flops | bytes accessed | tf_op | source)
XLA Modules:
  0.0 195.7 jit_solution(4689819661096860212)
XLA Ops:
  0.0 194.1 %shard_map.73 = bf16[192,512]{1,0:T(8,128)(2,1)} custom-call(bf16[192,2048]{1,0:T(8,128)(2,1)} %tok_hbm.1, f32[1,2048]{1,0:T(1,128)} %bitcast.3, s32[4,192]{1,0:T(4,128)} %bitcast.4, f32[4,192]{1,0:T(4,128)} %bitcast.5, bf16[1,2048,256]{2,1,0:T(8,128)(2,1)} %wg_hbm.1, bf16[1,2048,256]{2,1,0:T(8,128)(2,1)} %wu_hbm.1, bf16[1,256,2048]{2,1,0:T(8,128)(2,1)} %wd_hbm.1), custom_call_target="tpu_custom_call" | custom-call | tf_op jit(solution)/shard_map/pallas_call | solution.py:429
  194.1 1.6 copy.9
